TPU v7x, 32 devices: a whole 2x2x4 slice. The times are simulated.
32 devices in a mesh: sp: 16 (over z, y, x), tp: 2 (over core).
Axes of the slice: x: 2, y: 2, z: 4, core: 2. Of those that a mesh axis runs over, the one named last changes fastest.
Arguments:
- residual_in: bfloat16 [4096, 2048], P('sp'), may hold values from -6 to 6
- mixer_input: bfloat16 [2048, 4096], P('tp', 'sp'), may hold values from -6 to 6
- branch_gate: bfloat16 [2048, 4096], P('tp', 'sp'), may hold values from -6 to 6
- conv_taps: bfloat16 [2048, 4], P('tp'), may hold values from -3 to 3
- recur_weight: bfloat16 [32, 64, 64], P('tp'), may hold values from -0.75 to 0.75
- admit_weight: bfloat16 [32, 64, 64], P('tp'), may hold values from -0.75 to 0.75
- decay_param: float32 [2048], P('tp'), may hold values from 4 to 16
- decay_extra: float32 [2048, 4096], P('tp', 'sp'), may hold values from -1 to 0
- out_weight: bfloat16 [2048, 2048], P('tp'), may hold values from -0.375 to 0.375
- norm_gain: bfloat16 [2048], replicated, may hold values from 0.099609375 to 1.8984375
- gate_weight: bfloat16 [2048, 5632], P('sp', 'tp'), may hold values from -0.125 to 0.125
- up_weight: bfloat16 [2048, 5632], P('sp', 'tp'), may hold values from -0.125 to 0.125
- down_weight: bfloat16 [2048, 5632], P('sp', 'tp'), may hold values from -0.15625 to 0.15625
Outputs:
- layer_out: bfloat16 [4096, 2048], P('sp')
All inputs are finite; a program needn't handle non-finite values.
Results may differ from a plain program's by a relative error of at most 0.019.
Values may be sent and summed in bfloat16 or wider, within the bound.
A program may use at most 128 MiB of HBM per device.

v0:
```python
import jax
import jax.numpy as jnp
from jax import lax
from jax.sharding import PartitionSpec as P


def from_behind(value, axis, by):
    count = lax.axis_size(axis)
    pairs = [(i, i + by) for i in range(count) if 0 <= i + by < count]
    return lax.ppermute(value, axis, pairs)


def entering(value, axis, combine, identity):
    count, mine = (lax.axis_size(axis), lax.axis_index(axis))
    everything = jax.tree.map(lambda part: lax.all_gather(part, axis), value)
    start = jax.tree.map(
        lambda part, zero: jnp.broadcast_to(jnp.asarray(zero, part.dtype), part.shape),
        value,
        identity,
    )

    def turn(k, before):
        reached = k < mine
        new = combine(before, jax.tree.map(lambda part: part[k], everything))
        return jax.tree.map(lambda a, b: jnp.where(reached, a, b), new, before)

    return lax.fori_loop(0, count, turn, start)


def block_gates(weight, signal):
    groups = weight.shape[0]
    grouped = signal.reshape(groups, weight.shape[1], signal.shape[1])
    mapped = jnp.einsum("gij,git->gjt", weight, grouped, preferred_element_type=jnp.float32)
    return jax.nn.sigmoid(mapped.reshape(signal.shape))


def link_pairs(earlier, latter):
    return (earlier[0] * latter[0], latter[0] * earlier[1] + latter[1])


def on_device(
    residual_in,
    mixer_input,
    branch_gate,
    conv_taps,
    recur_weight,
    admit_weight,
    decay_param,
    decay_extra,
    out_weight,
    norm_gain,
    gate_weight,
    up_weight,
    down_weight,
):
    tap_count = conv_taps.shape[1]
    length = mixer_input.shape[1]
    tail_cols = mixer_input[:, length - (tap_count - 1) :]
    before = from_behind(tail_cols, "sp", 1)
    padded = jnp.concatenate([before, mixer_input], axis=1).astype(jnp.float32)
    tap_values = conv_taps.astype(jnp.float32)
    conv_sum = jnp.zeros(mixer_input.shape, jnp.float32)
    for tap in range(tap_count):
        conv_sum = conv_sum + tap_values[:, tap : tap + 1] * padded[:, tap : tap + length]
    conv_out = conv_sum.astype(jnp.bfloat16)
    recur_gate = block_gates(recur_weight, conv_out)
    admit_gate = block_gates(admit_weight, conv_out)
    base_rate = jax.nn.softplus(-decay_param)[:, None]
    log_decay = -8.0 * recur_gate * base_rate + decay_extra
    decay_step = jnp.exp(log_decay)
    drive_term = jnp.sqrt(-jnp.expm1(2.0 * log_decay)) * admit_gate * conv_out.astype(jnp.float32)
    running, local_state = lax.associative_scan(link_pairs, (decay_step, drive_term), axis=1)
    block_ends = (running[:, -1], local_state[:, -1])
    identity = (jnp.ones_like(block_ends[0]), jnp.zeros_like(block_ends[1]))
    incoming = entering(block_ends, "sp", link_pairs, identity)
    states = local_state + running * incoming[1][:, None]
    gate_act = jax.nn.gelu(branch_gate.astype(jnp.float32), approximate=True)
    mixed_out = (states * gate_act).astype(jnp.bfloat16)
    row_count = residual_in.shape[0]
    partial_value = lax.dot_general(
        mixed_out, out_weight, (((0,), (0,)), ((), ())), preferred_element_type=jnp.float32
    )
    branch = lax.psum(partial_value.astype(jnp.bfloat16), "tp").astype(jnp.float32)
    middle = (residual_in.astype(jnp.float32) + branch).astype(jnp.bfloat16)
    middle_wide = middle.astype(jnp.float32)
    row_scale = lax.rsqrt(jnp.mean(middle_wide * middle_wide, axis=1, keepdims=True) + 1e-06)
    normed = (middle_wide * row_scale * norm_gain.astype(jnp.float32)).astype(jnp.bfloat16)
    gate_pre = jnp.dot(
        normed,
        lax.all_gather(gate_weight, "sp", axis=0, tiled=True),
        preferred_element_type=jnp.float32,
    )
    up_pre = jnp.dot(
        normed,
        lax.all_gather(up_weight, "sp", axis=0, tiled=True),
        preferred_element_type=jnp.float32,
    )
    down_whole = lax.all_gather(down_weight, "sp", axis=0, tiled=True)
    hidden = (jax.nn.silu(gate_pre) * up_pre).astype(jnp.bfloat16)
    share = row_count // lax.axis_size("tp")
    channel_out = lax.psum_scatter(
        lax.dot_general(
            hidden, down_whole, (((1,), (1,)), ((), ())), preferred_element_type=jnp.float32
        ).astype(jnp.bfloat16),
        "tp",
        scatter_dimension=0,
        tiled=True,
    ).astype(jnp.float32)
    first_row = lax.axis_index("tp") * share
    own_rows = lax.dynamic_slice_in_dim(middle, first_row, share, 0)
    layer_rows = (own_rows.astype(jnp.float32) + channel_out).astype(jnp.bfloat16)
    return lax.all_gather(layer_rows, "tp", axis=0, tiled=True)


def solution(mesh):
    placed = (
        P("sp", None),
        P("tp", "sp"),
        P("tp", "sp"),
        P("tp", None),
        P("tp", None, None),
        P("tp", None, None),
        P("tp"),
        P("tp", "sp"),
        P("tp", None),
        P(),
        P("sp", "tp"),
        P("sp", "tp"),
        P("sp", "tp"),
    )
    return jax.shard_map(
        on_device, mesh=mesh, in_specs=placed, out_specs=P("sp", None), check_vma=False
    )
```

profile of v0, /device:TPU:25, one launch (start us, length us, event | category | flops | bytes accessed | tf_op | source)
XLA Modules:
  0.0 1465.7 jit_solution(1467909552372036297)
XLA Ops:
  13.2 6.2 collective-permute-done
  26.4 19.5 %slice.275 = f32[1024,128]{1,0:T(8,128)S(1)} slice(f32[1024,256]{1,0:T(8,128)S(1)} %get-tuple-element.132), slice={[0:1024:1], [0:255:2]} | slice | bytes 1048576 | tf_op jit(solution)/shard_map/slice | solution.py:72
  46.0 19.6 %slice.276 = f32[1024,128]{1,0:T(8,128)S(1)} slice(f32[1024,256]{1,0:T(8,128)S(1)} %get-tuple-element.132), slice={[0:1024:1], [1:256:2]} | slice | bytes 1048576 | tf_op jit(solution)/shard_map/slice | solution.py:72
  65.6 20.0 %slice.274 = f32[1024,128]{1,0:T(8,128)} slice(f32[1024,256]{1,0:T(8,128)S(1)} %get-tuple-element.133), slice={[0:1024:1], [1:256:2]} | slice | bytes 1048576 | tf_op jit(solution)/shard_map/slice | solution.py:72
  85.6 20.4 %slice.278 = f32[1024,128]{1,0:T(8,128)} slice(f32[1024,256]{1,0:T(8,128)S(1)} %get-tuple-element.133), slice={[0:1024:1], [0:255:2]} | slice | bytes 1048576 | tf_op jit(solution)/shard_map/slice | solution.py:72
  107.3 10.1 slice.281
  117.4 10.9 slice.282
  128.3 11.3 slice.280
  139.6 10.5 slice.284
  151.4 5.8 slice.287
  157.3 5.9 slice.288
  163.2 6.0 slice.286
  169.2 6.0 slice.290
  193.7 4.2 slice.299
  197.9 4.3 slice.300
  202.2 4.3 slice.298
  206.5 4.2 slice.302
  213.3 3.8 slice.305
  217.1 3.9 slice.306
  221.0 3.9 slice.304
  225.0 3.8 slice.308
  235.1 3.7 slice.312
  238.8 3.8 slice.310
  252.5 3.8 slice.303
  256.4 3.8 slice.320
  260.2 4.2 slice.297
  264.4 4.2 slice.322
  275.7 5.8 slice.285
  281.5 5.8 slice.326
  287.3 11.1 slice.279
  298.4 11.4 slice.328
  309.7 20.5 %slice.273 = f32[1024,127]{1,0:T(8,128)} slice(f32[1024,256]{1,0:T(8,128)} %copy-done.6), slice={[0:1024:1], [2:256:2]} | slice | bytes 1040384 | tf_op jit(solution)/shard_map/slice | solution.py:72
  330.3 20.5 %slice.330 = f32[1024,127]{1,0:T(8,128)} slice(f32[1024,256]{1,0:T(8,128)} %copy-done.7), slice={[0:1024:1], [2:256:2]} | slice | bytes 1040384 | tf_op jit(solution)/shard_map/slice | solution.py:72
  407.4 3.9 pad.121
  411.3 3.9 pad.105
  419.9 3.7 pad.104
  433.1 4.9 pad.123
  440.0 4.8 pad.106
  444.8 4.9 pad.107
  455.1 4.3 pad.124
  459.3 4.4 pad.125
  463.7 5.7 pad.109
  471.4 5.3 pad.108
  479.8 8.6 pad.110
  488.3 9.1 pad.111
  497.5 17.4 %pad.113 = f32[1024,256]{1,0:T(8,128)S(1)} pad(f32[1024,128]{1,0:T(8,128)S(1)} %add.282, f32[]{:T(128)} %constant.47.clone.1), padding=0_0_0x1_0_1 | pad | bytes 1572868 | tf_op jit(solution)/shard_map/pad | solution.py:72
  516.2 8.8 pad.126
  525.0 10.2 pad.127
  538.4 17.4 %pad.112 = f32[1024,256]{1,0:T(8,128)S(1)} pad(f32[1024,128]{1,0:T(8,128)S(1)} %pad_maximum_fusion.3, f32[]{:T(128)} %constant.47.clone.1), padding=0_0_0x0_1_1 | pad | bytes 1572868 | tf_op jit(solution)/shard_map/pad | solution.py:72
  556.1 175.3 %all-gather.1 = f32[16384,1]{1,0:T(8,128)} all-gather(f32[1024,1]{1,0:T(8,128)S(1)} %slice_add_fusion), channel_id=3, replica_groups=mesh['sp'=16,'tp'=2] {'sp'}, dimensions={0}, use_global_device_ids=true | all-gather | bytes 69632 | tf_op jit(solution)/shard_map/all_gather | solution.py:15
  731.4 4.7 reduce.1
  736.1 19.9 %pad.129 = f32[1024,256]{1,0:T(8,128)} pad(f32[1024,128]{1,0:T(8,128)S(1)} %copy-done.27, f32[]{:T(128)} %constant.47.clone.1), padding=0_0_0x1_0_1 | pad | bytes 1572868 | tf_op jit(solution)/shard_map/pad | solution.py:72
  757.3 19.9 %pad.128 = f32[1024,256]{1,0:T(8,128)} pad(f32[1024,128]{1,0:T(8,128)S(1)} %pad_maximum_fusion.10, f32[]{:T(128)} %constant.47.clone.1), padding=0_0_0x0_1_1 | pad | bytes 1572868 | tf_op jit(solution)/shard_map/pad | solution.py:72
  778.7 189.7 %all-gather = f32[16384,1]{1,0:T(8,128)} all-gather(f32[1024,1]{1,0:T(8,128)S(1)} %slice_add_fusion.1), channel_id=2, replica_groups=mesh['sp'=16,'tp'=2] {'sp'}, dimensions={0}, use_global_device_ids=true | all-gather | bytes 69632 | tf_op jit(solution)/shard_map/all_gather | solution.py:15
  968.5 4.8 reduce
  974.3 5.4 convolution_convert_fusion.1
  981.5 30.7 %all-reduce.34.cloned.1.call-done = bf16[256,2048]{1,0:T(8,128)(2,1)} async-done(((bf16[256,2048]{1,0:T(8,128)(2,1)}), bf16[256,2048]{1,0:T(8,128)(2,1)}) %all-reduce.34.cloned.1.call-update) | async-done | bytes 1048592 | tf_op jit(solution)/shard_map/psum | solution.py:83
  1013.9 120.5 %all-gather.7.cloned.1.call-done = bf16[2048,2816]{1,0:T(8,128)(2,1)} async-done(((bf16[128,2816]{1,0:T(8,128)(2,1)}), bf16[2048,2816]{1,0:T(8,128)(2,1)}) %all-gather.7.cloned.1.call-update) | async-done | bytes 11534352 | tf_op jit(solution)/shard_map/all_gather | solution.py:90
  1134.5 9.1 fusion.35
  1143.6 132.9 %all-gather.11.cloned.1.call-done = bf16[2048,2816]{1,0:T(8,128)(2,1)} async-done(((bf16[128,2816]{1,0:T(8,128)(2,1)}), bf16[2048,2816]{1,0:T(8,128)(2,1)}) %all-gather.11.cloned.1.call-update) | async-done | bytes 11534352 | tf_op jit(solution)/shard_map/all_gather | solution.py:98
  1276.5 142.0 %all-gather.9.cloned.1.call-done = bf16[2048,2816]{1,0:T(8,128)(2,1)} async-done(((bf16[128,2816]{1,0:T(8,128)(2,1)}), bf16[2048,2816]{1,0:T(8,128)(2,1)}) %all-gather.9.cloned.1.call-update) | async-done | bytes 11534352 | tf_op jit(solution)/shard_map/all_gather | solution.py:95
  1418.5 15.6 %convolution_convert_fusion = bf16[256,2048]{1,0:T(8,128)(2,1)} fusion(bf16[2048,2816]{1,0:T(8,128)(2,1)} %all-gather.11.cloned.1.call-done, bf16[2048,2816]{1,0:T(8,128)(2,1)} %all-gather.9.cloned.1.call-done, f32[256,2816]{1,0:T(8,128)} %fusion.35, bf16[256,2048]{1,0:T(8,128)(2,1)S(1)} %get-tuple-element.129, f32[2048]{0:T(1024)S(1)} %convert_element_type.66, ...), kind=kOutput, calls=%fused_computation.7 | convolution fusion | flops 5912526848 | bytes 28058624 | tf_op jit(solution)/shard_map/dot_general | solution.py:102
  1434.2 9.2 reduce-scatter.2.cloned.1.call-done
  1445.5 10.4 all-gather.13.cloned.1.call-done
  (223 shorter events, 159.8 us)
Async XLA Ops:
  7.4 15.0 %copy-start = (bf16[16,64,64]{2,1,0:T(8,128)(2,1)S(1)}, bf16[16,64,64]{2,1,0:T(8,128)(2,1)}, u32[]{:S(2)}) copy-start(bf16[16,64,64]{2,1,0:T(8,128)(2,1)} %param.20) | copy-start | bytes 393220
  7.4 1004.8 %all-reduce.34.cloned.1.call-start = ((), (), s32[]{:S(2)}) async-start(), calls=%async_computation.1 | async-start | bytes 2097152 | tf_op jit(solution)/shard_map/psum | solution.py:83
  8.5 10.9 collective-permute-start
  22.3 1.0 copy-start.40
  23.3 1.2 copy-start.36
  26.4 59.1 %copy-start.6 = (f32[1024,256]{1,0:T(8,128)}, f32[1024,256]{1,0:T(8,128)S(1)}, u32[]{:S(2)}) copy-start(f32[1024,256]{1,0:T(8,128)S(1)} %get-tuple-element.133) | copy-start | bytes 3145732
  26.4 80.9 %copy-start.7 = (f32[1024,256]{1,0:T(8,128)}, f32[1024,256]{1,0:T(8,128)S(1)}, u32[]{:S(2)}) copy-start(f32[1024,256]{1,0:T(8,128)S(1)} %get-tuple-element.132) | copy-start | bytes 3145732
  247.9 1.0 copy-start.4
  247.9 1.2 copy-start.5
  373.3 4.3 copy-start.8
  373.3 4.3 copy-start.9
  373.3 4.3 copy-start.12
  373.3 4.3 copy-start.14
  373.3 4.3 copy-start.26
  375.5 3.1 copy-start.3
  397.5 4.4 copy-start.10
  397.5 4.4 copy-start.11
  397.5 4.4 copy-start.13
  397.5 4.4 copy-start.15
  397.5 4.4 copy-start.25
  399.7 3.1 copy-start.2
  423.6 4.3 copy-start.16
  423.6 4.3 copy-start.17
  423.6 4.3 copy-start.18
  423.6 4.3 copy-start.21
  423.6 4.3 copy-start.34
  423.6 4.3 copy-start.35
  440.0 13.8 copy-start.19
  449.7 4.1 copy-start.20
  449.7 4.1 copy-start.22
  449.7 4.1 copy-start.32
  449.7 4.1 copy-start.33
  454.8 4.5 copy-start.28
  476.8 1.7 copy-start.30
  476.8 1.7 copy-start.31
  479.5 8.8 copy-start.29
  535.2 3.0 copy-start.24
  731.4 4.7 copy-start.27
  731.4 24.7 %copy-start.23 = (f32[1024,1]{1,0:T(8,128)S(1)}, f32[1024,1]{1,0:T(8,128)}, u32[]{:S(2)}) copy-start(f32[1024,1]{1,0:T(8,128)} %slice.382) | copy-start | bytes 12292
  968.5 5.8 copy-start.38
  979.7 1.8 copy-start.39
  979.7 32.5 %copy-start.37 = (bf16[256,2048]{1,0:T(8,128)(2,1)S(1)}, bf16[256,2048]{1,0:T(8,128)(2,1)}, u32[]{:S(2)}) copy-start(bf16[256,2048]{1,0:T(8,128)(2,1)} %param.15) | copy-start | bytes 3145732
  979.7 154.8 %all-gather.7.cloned.1.call-start = ((), (), s32[]{:S(2)}) async-start(), calls=%async_computation.2 | async-start | bytes 12255232 | tf_op jit(solution)/shard_map/all_gather | solution.py:90
  980.3 296.2 %all-gather.11.cloned.1.call-start = ((), (), s32[]{:S(2)}) async-start(), calls=%async_computation.4 | async-start | bytes 12255232 | tf_op jit(solution)/shard_map/all_gather | solution.py:98
  980.9 437.6 %all-gather.9.cloned.1.call-start = ((), (), s32[]{:S(2)}) async-start(), calls=%async_computation.3 | async-start | bytes 12255232 | tf_op jit(solution)/shard_map/all_gather | solution.py:95
  981.5 462.0 %reduce-scatter.2.cloned.1.call-start = ((), (), s32[]{:S(2)}) async-start(), calls=%async_computation.5 | async-start | bytes 1572864 | tf_op jit(solution)/shard_map/reduce_scatter | solution.py:101
  1418.5 39.7 %copy-start.1 = (bf16[16,64,64]{2,1,0:T(8,128)(2,1)S(1)}, bf16[16,64,64]{2,1,0:T(8,128)(2,1)}, u32[]{:S(2)}) copy-start(bf16[16,64,64]{2,1,0:T(8,128)(2,1)} %param.20) | copy-start | bytes 393220
  1434.2 21.7 %all-gather.13.cloned.1.call-start = ((), (), s32[]{:S(2)}) async-start(), calls=%async_computation.6 | async-start | bytes 1572864 | tf_op jit(solution)/shard_map/all_gather | solution.py:112
Sparse Core Ops, SparseCore 0:
  979.8 32.3 all-reduce.33
  1434.3 9.1 reduce-scatter.1
  1445.6 10.2 all-gather.12
Sparse Core Ops, SparseCore 1:
  982.9 151.5 all-gather.6
  1137.1 139.3 all-gather.10
  1279.1 139.3 all-gather.8
where the time goes:
time: 1480 us; the launch traced here: 1470 us
  local copies, waits for them, and re-layouts  519 us (35%)
  waiting for transfers between devices  454 us (31%)
  blocking collectives  365 us (25%)
  other arithmetic  77.5 us (5%)
  matrix products  31.1 us (2%)
  between operations  15.6 us (1%)
    all_gather x2, blocking collectives, entering(): everything = jax.tree.map(lambda part: lax.all_gather(part, axis), value)  365 us
    slice x42, local copies, waits for them, and re-layouts, on_device(): lax.associative_scan(link_pairs, (decay_step, drive_term), axis=1)  310 us
    pad x28, local copies, waits for them, and re-layouts, on_device(): lax.associative_scan(link_pairs, (decay_step, drive_term), axis=1)  188 us
    all_gather x1, waiting for transfers between devices, on_device(): lax.all_gather(up_weight, 'sp', axis=0, tiled=True)  142 us
    all_gather x1, waiting for transfers between devices, on_device(): down_whole = lax.all_gather(down_weight, 'sp', axis=0, tiled=True)  133 us
    all_gather x1, waiting for transfers between devices, on_device(): lax.all_gather(gate_weight, 'sp', axis=0, tiled=True)  121 us
    psum x1, waiting for transfers between devices, on_device(): lax.psum(partial_value.astype(jnp.bfloat16), 'tp').astype(jnp.float32)  30.7 us
  transfers between devices with their start and end apart: 7, of which 7 were waited for; matrix products, arithmetic and copies ran while one was open for 1% of the time, Pallas kernels for 0%

commit v1 on v0

v1 whole, which is shorter than its diff:
```python
import functools

import jax
import jax.numpy as jnp
from jax import lax
from jax.experimental import pallas as pl
from jax.experimental.pallas import tpu as pltpu
from jax.sharding import PartitionSpec as P

MESH = pl.DeviceIdType.MESH
LANES = 128


def neg_expm1(v):
    series = jnp.full_like(v, 1.0)
    for k in range(9, 1, -1):
        series = 1.0 + series * v * (1.0 / k)
    return jnp.where(v > -0.5, -v * series, 1.0 - jnp.exp(v))


def mixer_kernel(
    n,
    x_ref,
    halo_ref,
    bg_ref,
    extra_ref,
    taps_ref,
    rate_ref,
    wr_ref,
    wa_ref,
    out_ref,
    state_s,
    run_s,
    ends_s,
    all_s,
    in_s,
    send_sem,
    recv_sem,
):
    me = lax.axis_index("sp")
    barrier = pltpu.get_barrier_semaphore()

    def greet(k, carry):
        pl.semaphore_signal(
            barrier, inc=1, device_id={"sp": lax.rem(me + k, n)}, device_id_type=MESH
        )
        return carry

    lax.fori_loop(1, n, greet, 0)
    channels, length = x_ref.shape
    block = wr_ref.shape[1]
    groups = channels // LANES
    tap_count = taps_ref.shape[1]
    lane = lax.broadcasted_iota(jnp.int32, (LANES, length), 1)

    def local(g, carry):
        rows = pl.ds(pl.multiple_of(g * LANES, LANES), LANES)
        wide = jnp.concatenate(
            [halo_ref[rows, :].astype(jnp.float32), x_ref[rows, :].astype(jnp.float32)], axis=1
        )
        taps = taps_ref[rows, :]
        total = taps[:, tap_count - 1 :] * wide[:, LANES:]
        for tap in range(tap_count - 2, -1, -1):
            total = total + taps[:, tap : tap + 1] * pltpu.roll(wide, tap_count - 1 - tap, 1)[:, LANES:]
        conv = total.astype(jnp.bfloat16)
        per = LANES // block
        recur, admit = [], []
        for b in range(per):
            part = conv[b * block : (b + 1) * block]
            recur.append(jnp.dot(wr_ref[g * per + b], part, preferred_element_type=jnp.float32))
            admit.append(jnp.dot(wa_ref[g * per + b], part, preferred_element_type=jnp.float32))
        recur = jax.nn.sigmoid(jnp.concatenate(recur, axis=0))
        admit = jax.nn.sigmoid(jnp.concatenate(admit, axis=0))
        log_decay = recur * rate_ref[rows, :] + extra_ref[rows, :]
        a = jnp.exp(log_decay)
        b = jnp.sqrt(neg_expm1(2.0 * log_decay)) * admit * conv.astype(jnp.float32)
        shift = 1
        while shift < length:
            seen = lane >= shift
            b = b + a * jnp.where(seen, pltpu.roll(b, shift, 1), 0.0)
            a = a * jnp.where(seen, pltpu.roll(a, shift, 1), 1.0)
            shift *= 2
        state_s[rows, :] = b
        run_s[rows, :] = a
        ends_s[pl.ds(g, 1), :] = a[:, length - LANES :].T[LANES - 1 :]
        ends_s[pl.ds(groups + g, 1), :] = b[:, length - LANES :].T[LANES - 1 :]
        return carry

    lax.fori_loop(0, groups, local, 0)
    pl.semaphore_wait(barrier, n - 1)

    def copy_to(k):
        return pltpu.make_async_remote_copy(
            src_ref=ends_s,
            dst_ref=all_s.at[k - 1],
            send_sem=send_sem.at[k - 1],
            recv_sem=recv_sem.at[k - 1],
            device_id={"sp": lax.rem(me + k, n)},
            device_id_type=MESH,
        )

    def send(k, carry):
        copy_to(k).start()
        return carry

    lax.fori_loop(1, n, send, 0)

    def finish(k, carry):
        copy_to(k).wait()
        return carry

    lax.fori_loop(1, n, finish, 0)

    def fold(i, before):
        k = n - 1 - i
        part = all_s[k - 1]
        new = part[:groups] * before + part[groups:]
        return jnp.where(k <= me, new, before)

    in_s[...] = lax.fori_loop(0, n - 1, fold, jnp.zeros((groups, LANES), jnp.float32))

    def close(g, carry):
        rows = pl.ds(pl.multiple_of(g * LANES, LANES), LANES)
        entering = jnp.broadcast_to(in_s[pl.ds(g, 1), :], (LANES, LANES)).T
        entering = jnp.concatenate([entering] * (length // LANES), axis=1)
        states = state_s[rows, :] + run_s[rows, :] * entering
        v = bg_ref[rows, :].astype(jnp.float32)
        act = 0.5 * v * (1.0 + jnp.tanh(0.7978845608028654 * (v + 0.044715 * v * v * v)))
        out_ref[rows, :] = (states * act).astype(jnp.bfloat16)
        return carry

    lax.fori_loop(0, groups, close, 0)


def mixer(n, x, halo, bg, extra, taps, rate, wr, wa):
    channels, length = x.shape
    groups = channels // LANES
    vmem = pl.BlockSpec(memory_space=pltpu.VMEM)
    return pl.pallas_call(
        functools.partial(mixer_kernel, n),
        out_shape=jax.ShapeDtypeStruct((channels, length), jnp.bfloat16),
        in_specs=[vmem] * 8,
        out_specs=vmem,
        scratch_shapes=[
            pltpu.VMEM((channels, length), jnp.float32),
            pltpu.VMEM((channels, length), jnp.float32),
            pltpu.VMEM((2 * groups, LANES), jnp.float32),
            pltpu.VMEM((n - 1, 2 * groups, LANES), jnp.float32),
            pltpu.VMEM((groups, LANES), jnp.float32),
            pltpu.SemaphoreType.DMA((n - 1,)),
            pltpu.SemaphoreType.DMA((n - 1,)),
        ],
        compiler_params=pltpu.CompilerParams(
            collective_id=0, has_side_effects=True, vmem_limit_bytes=24 << 20
        ),
        cost_estimate=pl.CostEstimate(
            flops=200 * channels * length, bytes_accessed=12 * channels * length, transcendentals=0
        ),
        name="mixer",
    )(x, halo, bg, extra, taps, rate, wr, wa)


def on_device(
    residual_in,
    mixer_input,
    branch_gate,
    conv_taps,
    recur_weight,
    admit_weight,
    decay_param,
    decay_extra,
    out_weight,
    norm_gain,
    gate_weight,
    up_weight,
    down_weight,
):
    n = lax.axis_size("sp")
    length = mixer_input.shape[1]
    halo = lax.ppermute(
        mixer_input[:, length - LANES :], "sp", [(i, i + 1) for i in range(n - 1)]
    )
    rate = -8.0 * jax.nn.softplus(-decay_param)[:, None]
    mixed_out = mixer(
        n,
        mixer_input,
        halo,
        branch_gate,
        decay_extra,
        conv_taps.astype(jnp.float32),
        rate,
        recur_weight.transpose(0, 2, 1),
        admit_weight.transpose(0, 2, 1),
    )
    row_count = residual_in.shape[0]
    partial_value = lax.dot_general(
        mixed_out, out_weight, (((0,), (0,)), ((), ())), preferred_element_type=jnp.float32
    )
    branch = lax.psum(partial_value.astype(jnp.bfloat16), "tp").astype(jnp.float32)
    middle = (residual_in.astype(jnp.float32) + branch).astype(jnp.bfloat16)
    middle_wide = middle.astype(jnp.float32)
    row_scale = lax.rsqrt(jnp.mean(middle_wide * middle_wide, axis=1, keepdims=True) + 1e-06)
    normed = (middle_wide * row_scale * norm_gain.astype(jnp.float32)).astype(jnp.bfloat16)
    gate_pre = jnp.dot(
        normed,
        lax.all_gather(gate_weight, "sp", axis=0, tiled=True),
        preferred_element_type=jnp.float32,
    )
    up_pre = jnp.dot(
        normed,
        lax.all_gather(up_weight, "sp", axis=0, tiled=True),
        preferred_element_type=jnp.float32,
    )
    down_whole = lax.all_gather(down_weight, "sp", axis=0, tiled=True)
    hidden = (jax.nn.silu(gate_pre) * up_pre).astype(jnp.bfloat16)
    share = row_count // lax.axis_size("tp")
    channel_out = lax.psum_scatter(
        lax.dot_general(
            hidden, down_whole, (((1,), (1,)), ((), ())), preferred_element_type=jnp.float32
        ).astype(jnp.bfloat16),
        "tp",
        scatter_dimension=0,
        tiled=True,
    ).astype(jnp.float32)
    first_row = lax.axis_index("tp") * share
    own_rows = lax.dynamic_slice_in_dim(middle, first_row, share, 0)
    layer_rows = (own_rows.astype(jnp.float32) + channel_out).astype(jnp.bfloat16)
    return lax.all_gather(layer_rows, "tp", axis=0, tiled=True)


def solution(mesh):
    placed = (
        P("sp", None),
        P("tp", "sp"),
        P("tp", "sp"),
        P("tp", None),
        P("tp", None, None),
        P("tp", None, None),
        P("tp"),
        P("tp", "sp"),
        P("tp", None),
        P(),
        P("sp", "tp"),
        P("sp", "tp"),
        P("sp", "tp"),
    )
    return jax.shard_map(
        on_device, mesh=mesh, in_specs=placed, out_specs=P("sp", None), check_vma=False
    )
```

time: 1480 us -> 514 us (0.35)
  local copies, waits for them, and re-layouts: 519 us -> 8.49 us
  blocking collectives: 365 us -> 0 us
  other arithmetic: 77.5 us -> 4.43 us
    all_gather x2 -> x0, blocking collectives: 365 us -> none  [entering(): everything = jax.tree.map(lambda part: lax.all_gather(part, axis), value)]
    slice x44 -> x1, local copies, waits for them, and re-layouts: 312 us -> 1.79 us  [on_device(): mixer_input[:, length - LANES:]]
    pad x28 -> x0, local copies, waits for them, and re-layouts: 188 us -> none  [on_device(): lax.associative_scan(link_pairs, (decay_step, drive_term), axis=1)]
    add x30 -> x0, other arithmetic: 42.1 us -> none  [the longest x15 22.8 us: on_device(): lax.associative_scan(link_pairs, (decay_step, drive_term), axis=1)]
  transfers between devices with their start and end apart: 7 -> 7, of which waited for: 7 -> 7; matrix products, arithmetic and copies ran while one was open for 1% -> 3% of each run, Pallas kernels for 0% -> 0%
where the time goes in v1:
time: 514 us; the launch traced here: 513 us
  waiting for transfers between devices  441 us (86%)
  matrix products  27 us (5%)
  between operations  14.9 us (3%)
  Pallas kernels  13.3 us (3%)
  local copies, waits for them, and re-layouts  8.49 us (2%)
    all_gather x1, waiting for transfers between devices, on_device(): down_whole = lax.all_gather(down_weight, 'sp', axis=0, tiled=True)  142 us
    all_gather x1, waiting for transfers between devices, on_device(): lax.all_gather(up_weight, 'sp', axis=0, tiled=True)  133 us
    all_gather x1, waiting for transfers between devices, on_device(): lax.all_gather(gate_weight, 'sp', axis=0, tiled=True)  121 us
    psum x1, waiting for transfers between devices, on_device(): lax.psum(partial_value.astype(jnp.bfloat16), 'tp').astype(jnp.float32)  20.8 us
    dot_general x1, matrix products, on_device(): lax.dot_general(hidden, down_whole, (((1,), (1,)), ((), ())), preferred_e...  15.6 us
    pallas_call x1, Pallas kernels, mixer(): pl.pallas_call(functools.partial(mixer_kernel, n), out_shape=jax.ShapeDty...  13.3 us
    all_gather x1, waiting for transfers between devices, on_device(): return lax.all_gather(layer_rows, 'tp', axis=0, tiled=True)  10.4 us
  transfers between devices with their start and end apart: 7, of which 7 were waited for; matrix products, arithmetic and copies ran while one was open for 3% of the time, Pallas kernels for 0%

profile of v1, /device:TPU:25, one launch (start us, length us, event | category | flops | bytes accessed | tf_op | source)
XLA Modules:
  0.0 512.8 jit_solution(12299645158734164411)
XLA Ops:
  7.4 0.0 copy-start
  7.4 0.0 copy-start.1
  7.4 0.0 all-reduce.2.cloned.1.call-start
  7.4 1.8 slice.3
  9.2 3.1 collective-permute-start
  12.3 0.7 fusion.8
  13.0 0.2 copy.24.rate_ref
  13.2 0.9 copy.23.taps_ref
  14.1 1.1 copy.21
  15.2 1.1 copy.22
  16.3 3.9 collective-permute-done.halo_ref
  20.2 0.0 copy-done
  20.2 0.0 copy-done.1
  20.2 0.0 copy-start.2
  20.2 1.0 copy-done.2
  21.3 0.0 copy-start.5
  21.3 13.3 %mixer.1 = bf16[1024,256]{1,0:T(8,128)(2,1)S(1)} custom-call(bf16[1024,256]{1,0:T(8,128)(2,1)S(1)} %copy-done, bf16[1024,128]{1,0:T(8,128)(2,1)S(1)} %collective-permute-done.halo_ref, bf16[1024,256]{1,0:T(8,128)(2,1)S(1)} %copy-done.2, f32[1024,256]{1,0:T(8,128)S(1)} %copy-done.1, f32[1024,4]{1,0:T(8,128)S(1)} %copy.23.taps_ref, ...), custom_call_target="tpu_custom_call" | custom-call | flops 52428800 | bytes 3145728 | tf_op jit(solution)/shard_map/mixer/pallas_call | solution.py:139
  34.6 0.0 copy-done.5
  34.6 2.2 convolution_convert_fusion.1
  36.8 0.0 copy-start.4
  36.8 0.0 copy-start.3
  36.8 0.0 all-reduce.2.cloned.1.call-update
  36.9 0.0 all-gather.5.cloned.1.call-start
  36.9 0.5 all-gather.5.cloned.1.call-update
  37.4 0.0 all-gather.7.cloned.1.call-start
  37.5 0.5 all-gather.7.cloned.1.call-update
  38.0 0.0 all-gather.9.cloned.1.call-start
  38.1 0.5 all-gather.9.cloned.1.call-update
  38.6 0.0 reduce-scatter.2.cloned.1.call-start
  38.7 0.0 copy-done.4
  38.7 20.8 %all-reduce.2.cloned.1.call-done = bf16[256,2048]{1,0:T(8,128)(2,1)} async-done(((bf16[256,2048]{1,0:T(8,128)(2,1)}), bf16[256,2048]{1,0:T(8,128)(2,1)}) %all-reduce.2.cloned.1.call-update) | async-done | bytes 1048592 | tf_op jit(solution)/shard_map/psum | solution.py:199
  59.5 0.0 copy-done.3
  59.5 1.8 fusion.1
  61.3 120.5 %all-gather.5.cloned.1.call-done = bf16[2048,2816]{1,0:T(8,128)(2,1)} async-done(((bf16[128,2816]{1,0:T(8,128)(2,1)}), bf16[2048,2816]{1,0:T(8,128)(2,1)}) %all-gather.5.cloned.1.call-update) | async-done | bytes 11534352 | tf_op jit(solution)/shard_map/all_gather | solution.py:206
  181.8 9.1 %fusion.6 = f32[256,2816]{1,0:T(8,128)} fusion(bf16[2048,2816]{1,0:T(8,128)(2,1)} %all-gather.5.cloned.1.call-done, bf16[256,2048]{1,0:T(8,128)(2,1)S(1)} %get-tuple-element.6, f32[2048]{0:T(1024)S(1)} %convert_element_type.46, f32[256]{0:T(256)S(1)} %add_rsqrt_fusion), kind=kOutput, calls=%fused_computation.11 | convolution fusion | flops 2954887168 | bytes 15475712 | tf_op jit(solution)/shard_map/dot_general | solution.py:204
  191.0 132.9 %all-gather.7.cloned.1.call-done = bf16[2048,2816]{1,0:T(8,128)(2,1)} async-done(((bf16[128,2816]{1,0:T(8,128)(2,1)}), bf16[2048,2816]{1,0:T(8,128)(2,1)}) %all-gather.7.cloned.1.call-update) | async-done | bytes 11534352 | tf_op jit(solution)/shard_map/all_gather | solution.py:211
  323.9 142.0 %all-gather.9.cloned.1.call-done = bf16[2048,2816]{1,0:T(8,128)(2,1)} async-done(((bf16[128,2816]{1,0:T(8,128)(2,1)}), bf16[2048,2816]{1,0:T(8,128)(2,1)}) %all-gather.9.cloned.1.call-update) | async-done | bytes 11534352 | tf_op jit(solution)/shard_map/all_gather | solution.py:214
  465.9 15.6 %convolution_convert_fusion = bf16[256,2048]{1,0:T(8,128)(2,1)} fusion(bf16[2048,2816]{1,0:T(8,128)(2,1)} %all-gather.9.cloned.1.call-done, bf16[2048,2816]{1,0:T(8,128)(2,1)} %all-gather.7.cloned.1.call-done, f32[256,2816]{1,0:T(8,128)} %fusion.6, bf16[256,2048]{1,0:T(8,128)(2,1)S(1)} %get-tuple-element.6, f32[2048]{0:T(1024)S(1)} %convert_element_type.46, ...), kind=kOutput, calls=%fused_computation.4 | convolution fusion | flops 5912526848 | bytes 28058624 | tf_op jit(solution)/shard_map/dot_general | solution.py:218
  481.5 0.0 reduce-scatter.2.cloned.1.call-update
  481.5 0.0 all-gather.11.cloned.1.call-start
  481.6 9.2 %reduce-scatter.2.cloned.1.call-done = bf16[128,2048]{1,0:T(8,128)(2,1)} async-done(((bf16[256,2048]{1,0:T(8,128)(2,1)}), bf16[128,2048]{1,0:T(8,128)(2,1)}) %reduce-scatter.2.cloned.1.call-update) | async-done | bytes 524304 | tf_op jit(solution)/shard_map/reduce_scatter | solution.py:217
  490.8 2.0 add_convert_fusion.1
  492.8 0.0 all-gather.11.cloned.1.call-update
  492.8 10.4 %all-gather.11.cloned.1.call-done = bf16[256,2048]{1,0:T(8,128)(2,1)} async-done(((bf16[128,2048]{1,0:T(8,128)(2,1)}), bf16[256,2048]{1,0:T(8,128)(2,1)}) %all-gather.11.cloned.1.call-update) | async-done | bytes 1048592 | tf_op jit(solution)/shard_map/all_gather | solution.py:228
  503.2 2.3 copy.27
  (2 shorter events, 0.0 us)
Async XLA Ops:
  7.4 12.9 %copy-start = (bf16[1024,256]{1,0:T(8,128)(2,1)S(1)}, bf16[1024,256]{1,0:T(8,128)(2,1)}, u32[]{:S(2)}) copy-start(bf16[1024,256]{1,0:T(8,128)(2,1)} %x_ref.1) | copy-start | bytes 1572868
  7.4 12.9 %copy-start.1 = (f32[1024,256]{1,0:T(8,128)S(1)}, f32[1024,256]{1,0:T(8,128)}, u32[]{:S(2)}) copy-start(f32[1024,256]{1,0:T(8,128)} %extra_ref.1) | copy-start | bytes 3145732
  7.4 52.2 %all-reduce.2.cloned.1.call-start = ((), (), s32[]{:S(2)}) async-start(), calls=%async_computation.1 | async-start | bytes 2097152 | tf_op jit(solution)/shard_map/psum | solution.py:199
  9.2 11.1 %collective-permute-start = (bf16[1024,128]{1,0:T(8,128)(2,1)}, bf16[1024,128]{1,0:T(8,128)(2,1)S(1)}, u32[]{:S(2)}, u32[]{:S(2)}) collective-permute-start(bf16[1024,128]{1,0:T(8,128)(2,1)} %slice.3), channel_id=1, source_target_pairs={{0,2},{2,4},{4,6},{6,8},{8,10},{10,12},{12,14},{14,16},{16,18},{18... | collective-permute-start | bytes 786440 | tf_op jit(solution)/shard_map/ppermute | solution.py:180
  20.2 1.0 copy-start.2
  21.3 13.3 %copy-start.5 = (bf16[1024,2048]{1,0:T(8,128)(2,1)S(1)}, bf16[1024,2048]{1,0:T(8,128)(2,1)}, u32[]{:S(2)}) copy-start(bf16[1024,2048]{1,0:T(8,128)(2,1)} %param.21) | copy-start | bytes 12582916
  36.8 1.8 copy-start.4
  36.8 22.7 %copy-start.3 = (bf16[256,2048]{1,0:T(8,128)(2,1)S(1)}, bf16[256,2048]{1,0:T(8,128)(2,1)}, u32[]{:S(2)}) copy-start(bf16[256,2048]{1,0:T(8,128)(2,1)} %param.13) | copy-start | bytes 3145732
  36.9 145.0 %all-gather.5.cloned.1.call-start = ((), (), s32[]{:S(2)}) async-start(), calls=%async_computation.2 | async-start | bytes 12255232 | tf_op jit(solution)/shard_map/all_gather | solution.py:206
  37.4 286.4 %all-gather.7.cloned.1.call-start = ((), (), s32[]{:S(2)}) async-start(), calls=%async_computation.3 | async-start | bytes 12255232 | tf_op jit(solution)/shard_map/all_gather | solution.py:211
  38.0 427.8 %all-gather.9.cloned.1.call-start = ((), (), s32[]{:S(2)}) async-start(), calls=%async_computation.4 | async-start | bytes 12255232 | tf_op jit(solution)/shard_map/all_gather | solution.py:214
  38.6 452.2 %reduce-scatter.2.cloned.1.call-start = ((), (), s32[]{:S(2)}) async-start(), calls=%async_computation.5 | async-start | bytes 1572864 | tf_op jit(solution)/shard_map/reduce_scatter | solution.py:217
  481.5 21.7 %all-gather.11.cloned.1.call-start = ((), (), s32[]{:S(2)}) async-start(), calls=%async_computation.6 | async-start | bytes 1572864 | tf_op jit(solution)/shard_map/all_gather | solution.py:228
Sparse Core Ops, SparseCore 0:
  37.0 22.4 all-reduce.1
  481.6 9.1 reduce-scatter.1
  492.9 10.2 all-gather.10
Sparse Core Ops, SparseCore 1:
  40.1 141.7 all-gather.4
  184.5 139.3 all-gather.6
  326.5 139.3 all-gather.8

commit v2 on v1

--- a/solution.py
+++ b/solution.py
@@ -160,6 +160,457 @@
     )(x, halo, bg, extra, taps, rate, wr, wa)
 
 
+def layer_kernel(
+    n,
+    split,
+    x_ref,
+    halo_ref,
+    bg_ref,
+    extra_ref,
+    taps_ref,
+    rate_ref,
+    wr_ref,
+    wa_ref,
+    ow_ref,
+    res_ref,
+    gain_ref,
+    packed_ref,
+    wide_ref,
+    tok_ref,
+    mid_ref,
+    state_s,
+    run_s,
+    ends_s,
+    all_s,
+    in_s,
+    mix_s,
+    part_s,
+    part_r,
+    nrm_s,
+    own_s,
+    send_sem,
+    recv_sem,
+    zs_sem,
+    zr_sem,
+    ps_sem,
+    pr_sem,
+    fs_sem,
+    fr_sem,
+    ts_sem,
+    tr_sem,
+    bs_sem,
+    br_sem,
+    cs_sem,
+    cr_sem,
+    own_sem,
+):
+    me = lax.axis_index("sp")
+    core = lax.axis_index("tp")
+    plane = n // split
+    rank, spot = me // plane, lax.rem(me, plane)
+    barrier = pltpu.get_barrier_semaphore()
+
+    def greet(k, carry):
+        pl.semaphore_signal(
+            barrier, inc=1, device_id={"sp": lax.rem(me + k, n)}, device_id_type=MESH
+        )
+        return carry
+
+    lax.fori_loop(1, n, greet, 0)
+    pl.semaphore_signal(barrier, inc=1, device_id={"tp": 1 - core}, device_id_type=MESH)
+    pl.semaphore_wait(barrier, n)
+
+    depth = packed_ref.shape[3]
+    span = packed_ref.shape[2]
+    kinds = packed_ref.shape[1]
+
+    def columns(source):
+        return pl.ds(pl.multiple_of(source * depth, depth), depth)
+
+    def remote(src, dst, ssem, rsem, where):
+        return pltpu.make_async_remote_copy(
+            src_ref=src, dst_ref=dst, send_sem=ssem, recv_sem=rsem,
+            device_id=where, device_id_type=MESH,
+        )
+
+    def z_copy(c, k):
+        to = lax.rem(rank + k, split)
+        return remote(
+            packed_ref.at[to, c], wide_ref.at[c, :, columns(me)],
+            zs_sem.at[c, k - 1], zr_sem.at[c, k - 1], {"sp": to * plane + spot},
+        )
+
+    def z_landed(c, k):
+        source = lax.rem(rank - k + split, split) * plane + spot
+        return remote(
+            packed_ref.at[rank, c], wide_ref.at[c, :, columns(source)],
+            zs_sem.at[c, k - 1], zr_sem.at[c, k - 1], {"sp": source},
+        )
+
+    def own_copy(c, m):
+        return remote(
+            packed_ref.at[rank, c], wide_ref.at[c, :, columns(me)],
+            ps_sem.at[c, m - 1], pr_sem.at[c, m - 1],
+            {"sp": rank * plane + lax.rem(spot + m, plane)},
+        )
+
+    def own_landed(c, m):
+        source = rank * plane + lax.rem(spot - m + plane, plane)
+        return remote(
+            packed_ref.at[rank, c], wide_ref.at[c, :, columns(source)],
+            ps_sem.at[c, m - 1], pr_sem.at[c, m - 1], {"sp": source},
+        )
+
+    def pass_copy(c, k, m):
+        source = lax.rem(rank - k + split, split) * plane + spot
+        window = wide_ref.at[c, :, columns(source)]
+        return remote(
+            window, window, fs_sem.at[c, k - 1, m - 1], fr_sem.at[c, k - 1, m - 1],
+            {"sp": rank * plane + lax.rem(spot + m, plane)},
+        )
+
+    def pass_landed(c, k, m):
+        behind = lax.rem(spot - m + plane, plane)
+        source = lax.rem(rank - k + split, split) * plane + behind
+        window = wide_ref.at[c, :, columns(source)]
+        return remote(
+            window, window, fs_sem.at[c, k - 1, m - 1], fr_sem.at[c, k - 1, m - 1],
+            {"sp": rank * plane + behind},
+        )
+
+    def z_start(c):
+        for k in range(1, split):
+            z_copy(c, k).start()
+
+    def z_pass(c):
+        for k in range(1, split):
+            z_landed(c, k).wait_recv()
+            for m in range(1, plane):
+                pass_copy(c, k, m).start()
+
+    z_start(0)
+    for c in range(kinds):
+        for m in range(1, plane):
+            own_copy(c, m).start()
+    own_in = pltpu.make_async_copy(packed_ref.at[rank], own_s, own_sem.at[0])
+    own_in.start()
+    channels, length = x_ref.shape
+    block = wr_ref.shape[1]
+    groups = channels // LANES
+    tap_count = taps_ref.shape[1]
+    lane = lax.broadcasted_iota(jnp.int32, (LANES, length), 1)
+
+    def local(g, carry):
+        rows = pl.ds(pl.multiple_of(g * LANES, LANES), LANES)
+        wide = jnp.concatenate(
+            [halo_ref[rows, :].astype(jnp.float32), x_ref[rows, :].astype(jnp.float32)], axis=1
+        )
+        taps = taps_ref[rows, :]
+        total = taps[:, tap_count - 1 :] * wide[:, LANES:]
+        for tap in range(tap_count - 2, -1, -1):
+            total = total + taps[:, tap : tap + 1] * pltpu.roll(wide, tap_count - 1 - tap, 1)[:, LANES:]
+        conv = total.astype(jnp.bfloat16)
+        per = LANES // block
+        recur, admit = [], []
+        for b in range(per):
+            part = conv[b * block : (b + 1) * block]
+            recur.append(jnp.dot(wr_ref[g * per + b], part, preferred_element_type=jnp.float32))
+            admit.append(jnp.dot(wa_ref[g * per + b], part, preferred_element_type=jnp.float32))
+        recur = jax.nn.sigmoid(jnp.concatenate(recur, axis=0))
+        admit = jax.nn.sigmoid(jnp.concatenate(admit, axis=0))
+        log_decay = recur * rate_ref[rows, :] + extra_ref[rows, :]
+        a = jnp.exp(log_decay)
+        b = jnp.sqrt(neg_expm1(2.0 * log_decay)) * admit * conv.astype(jnp.float32)
+        shift = 1
+        while shift < length:
+            seen = lane >= shift
+            b = b + a * jnp.where(seen, pltpu.roll(b, shift, 1), 0.0)
+            a = a * jnp.where(seen, pltpu.roll(a, shift, 1), 1.0)
+            shift *= 2
+        state_s[rows, :] = b
+        run_s[rows, :] = a
+        ends_s[pl.ds(g, 1), :] = a[:, length - LANES :].T[LANES - 1 :]
+        ends_s[pl.ds(groups + g, 1), :] = b[:, length - LANES :].T[LANES - 1 :]
+        return carry
+
+    lax.fori_loop(0, groups, local, 0)
+
+    own_in.wait()
+    own_out = pltpu.make_async_copy(own_s, wide_ref.at[:, :, columns(me)], own_sem.at[1])
+    own_out.start()
+    z_pass(0)
+    z_start(1)
+    def copy_to(k):
+        return pltpu.make_async_remote_copy(
+            src_ref=ends_s,
+            dst_ref=all_s.at[k - 1],
+            send_sem=send_sem.at[k - 1],
+            recv_sem=recv_sem.at[k - 1],
+            device_id={"sp": lax.rem(me + k, n)},
+            device_id_type=MESH,
+        )
+
+    def send(k, carry):
+        copy_to(k).start()
+        return carry
+
+    lax.fori_loop(1, n, send, 0)
+
+    def finish(k, carry):
+        copy_to(k).wait()
+        return carry
+
+    lax.fori_loop(1, n, finish, 0)
+
+    def fold(i, before):
+        k = n - 1 - i
+        part = all_s[k - 1]
+        new = part[:groups] * before + part[groups:]
+        return jnp.where(k <= me, new, before)
+
+    in_s[...] = lax.fori_loop(0, n - 1, fold, jnp.zeros((groups, LANES), jnp.float32))
+
+    def close(g, carry):
+        rows = pl.ds(pl.multiple_of(g * LANES, LANES), LANES)
+        entering = jnp.broadcast_to(in_s[pl.ds(g, 1), :], (LANES, LANES)).T
+        entering = jnp.concatenate([entering] * (length // LANES), axis=1)
+        states = state_s[rows, :] + run_s[rows, :] * entering
+        v = bg_ref[rows, :].astype(jnp.float32)
+        act = 0.5 * v * (1.0 + jnp.tanh(0.7978845608028654 * (v + 0.044715 * v * v * v)))
+        mix_s[:, rows] = (states * act).T.astype(jnp.bfloat16)
+        return carry
+
+    lax.fori_loop(0, groups, close, 0)
+
+    pieces, row_count, cut = part_s.shape
+
+    def swap(i):
+        return remote(
+            part_s.at[i], part_r.at[i], bs_sem.at[i], br_sem.at[i], {"tp": 1 - core}
+        )
+
+    for i in range(pieces):
+        part_s[i] = jnp.dot(
+            mix_s[...], ow_ref[:, i * cut : (i + 1) * cut], preferred_element_type=jnp.float32
+        ).astype(jnp.bfloat16)
+        if i:
+            swap(i - 1).start()
+    z_pass(1)
+    z_start(2)
+    swap(pieces - 1).start()
+    square = jnp.zeros((row_count, 1), jnp.float32)
+    for i in range(pieces):
+        swap(i).wait()
+        cols = slice(i * cut, (i + 1) * cut)
+        branch = part_s[i].astype(jnp.float32) + part_r[i].astype(jnp.float32)
+        middle = (res_ref[:, cols].astype(jnp.float32) + branch).astype(jnp.bfloat16)
+        mid_ref[:, cols] = middle
+        middle = middle.astype(jnp.float32)
+        square = square + jnp.sum(middle * middle, axis=1, keepdims=True)
+    scale = lax.rsqrt(square * (1.0 / (pieces * cut)) + 1e-06)
+    for i in range(pieces):
+        cols = slice(i * cut, (i + 1) * cut)
+        middle = mid_ref[:, cols].astype(jnp.float32)
+        nrm_s[:, cols] = (middle * scale * gain_ref[:, cols].astype(jnp.float32)).astype(jnp.bfloat16)
+    half = row_count // 2
+    mine = pl.ds(pl.multiple_of(core * half, half), half)
+    other = pl.ds(pl.multiple_of((1 - core) * half, half), half)
+
+    def tok_copy(k):
+        to = lax.rem(rank + k, split)
+        return remote(
+            nrm_s.at[mine, :], tok_ref.at[rank, mine, :],
+            ts_sem.at[k - 1], tr_sem.at[k - 1], {"sp": to * plane + spot},
+        )
+
+    def tok_landed(k):
+        source = lax.rem(rank - k + split, split)
+        return remote(
+            nrm_s.at[mine, :], tok_ref.at[source, mine, :],
+            ts_sem.at[k - 1], tr_sem.at[k - 1], {"sp": source * plane + spot},
+        )
+
+    def tok_pass(k, rows):
+        source = lax.rem(rank - k + split, split)
+        window = tok_ref.at[source, rows, :]
+        return remote(window, window, cs_sem.at[k - 1], cr_sem.at[k - 1], {"tp": 1 - core})
+
+    for k in range(1, split):
+        tok_copy(k).start()
+    own_tok = pltpu.make_async_copy(nrm_s, tok_ref.at[rank], own_sem.at[2])
+    own_tok.start()
+    z_pass(2)
+    for k in range(1, split):
+        tok_landed(k).wait_recv()
+        tok_pass(k, mine).start()
+    for k in range(1, split):
+        tok_copy(k).wait_send()
+        tok_pass(k, mine).wait_send()
+        tok_pass(k, other).wait_recv()
+    own_tok.wait()
+    own_out.wait()
+    for c in range(kinds):
+        for m in range(1, plane):
+            own_copy(c, m).wait_send()
+            own_landed(c, m).wait_recv()
+        for k in range(1, split):
+            z_copy(c, k).wait_send()
+            for m in range(1, plane):
+                pass_copy(c, k, m).wait_send()
+                pass_landed(c, k, m).wait_recv()
+
+
+def layer_front(n, split, x, halo, bg, extra, taps, rate, wr, wa, ow, res, gain, packed):
+    channels, length = x.shape
+    groups = channels // LANES
+    rows, width = res.shape
+    kinds, span, depth = packed.shape[1:]
+    plane = n // split
+    cut = 512
+    pieces = width // cut
+    vmem = pl.BlockSpec(memory_space=pltpu.VMEM)
+    hbm = pl.BlockSpec(memory_space=pl.ANY)
+    dma = pltpu.SemaphoreType.DMA
+    bf16, f32 = jnp.bfloat16, jnp.float32
+    return pl.pallas_call(
+        functools.partial(layer_kernel, n, split),
+        out_shape=(
+            jax.ShapeDtypeStruct((kinds, span, n * depth), bf16),
+            jax.ShapeDtypeStruct((split, rows, width), bf16),
+            jax.ShapeDtypeStruct((rows, width), bf16),
+        ),
+        in_specs=[vmem] * 11 + [hbm],
+        out_specs=(hbm, hbm, vmem),
+        scratch_shapes=[
+            pltpu.VMEM((channels, length), f32),
+            pltpu.VMEM((channels, length), f32),
+            pltpu.VMEM((2 * groups, LANES), f32),
+            pltpu.VMEM((n - 1, 2 * groups, LANES), f32),
+            pltpu.VMEM((groups, LANES), f32),
+            pltpu.VMEM((length, channels), bf16),
+            pltpu.VMEM((pieces, rows, cut), bf16),
+            pltpu.VMEM((pieces, rows, cut), bf16),
+            pltpu.VMEM((rows, width), bf16),
+            pltpu.VMEM((kinds, span, depth), bf16),
+            dma((n - 1,)),
+            dma((n - 1,)),
+            dma((kinds, split - 1)),
+            dma((kinds, split - 1)),
+            dma((kinds, plane - 1)),
+            dma((kinds, plane - 1)),
+            dma((kinds, split - 1, plane - 1)),
+            dma((kinds, split - 1, plane - 1)),
+            dma((split - 1,)),
+            dma((split - 1,)),
+            dma((pieces,)),
+            dma((pieces,)),
+            dma((split - 1,)),
+            dma((split - 1,)),
+            dma((3,)),
+        ],
+        compiler_params=pltpu.CompilerParams(
+            collective_id=1, has_side_effects=True, vmem_limit_bytes=40 << 20
+        ),
+        name="layer_front",
+    )(x, halo, bg, extra, taps, rate, wr, wa, ow, res, gain, packed)
+
+
+def close_kernel(
+    n, split, part_ref, mid_ref, out_ref,
+    tp_s, red_s, z_s, half_s, half_r,
+    as_sem, ar_sem, zs_sem, zr_sem, hs_sem, hr_sem,
+):
+    me = lax.axis_index("sp")
+    core = lax.axis_index("tp")
+    plane = n // split
+    rank, spot = me // plane, lax.rem(me, plane)
+    barrier = pltpu.get_barrier_semaphore()
+    for k in range(1, split):
+        pl.semaphore_signal(
+            barrier, inc=1,
+            device_id={"sp": lax.rem(rank + k, split) * plane + spot}, device_id_type=MESH,
+        )
+    pl.semaphore_signal(barrier, inc=1, device_id={"tp": 1 - core}, device_id_type=MESH)
+    pl.semaphore_wait(barrier, split)
+    half = part_ref.shape[1] // 2
+    mine = pl.ds(pl.multiple_of(core * half, half), half)
+    other = pl.ds(pl.multiple_of((1 - core) * half, half), half)
+
+    def to_rank(k):
+        return lax.rem(rank + k, split)
+
+    def tp_copy(k):
+        return pltpu.make_async_remote_copy(
+            src_ref=part_ref.at[to_rank(k), other, :], dst_ref=tp_s.at[k],
+            send_sem=as_sem.at[k], recv_sem=ar_sem.at[k],
+            device_id={"tp": 1 - core}, device_id_type=MESH,
+        )
+
+    def z_copy(k):
+        return pltpu.make_async_remote_copy(
+            src_ref=red_s.at[k - 1], dst_ref=z_s.at[k - 1],
+            send_sem=zs_sem.at[k - 1], recv_sem=zr_sem.at[k - 1],
+            device_id={"sp": to_rank(k) * plane + spot}, device_id_type=MESH,
+        )
+
+    order = list(range(1, split)) + [0]
+    for k in order:
+        tp_copy(k).start()
+    for k in order[:-1]:
+        tp_copy(k).wait()
+        mixed = part_ref[to_rank(k), mine, :].astype(jnp.float32) + tp_s[k].astype(jnp.float32)
+        red_s[k - 1] = mixed.astype(jnp.bfloat16)
+        if k > 1:
+            z_copy(k - 1).start()
+    tp_copy(0).wait()
+    z_copy(split - 1).start()
+    total = part_ref[rank, mine, :].astype(jnp.float32) + tp_s[0].astype(jnp.float32)
+    for k in range(1, split):
+        z_copy(k).wait()
+        total = total + z_s[k - 1].astype(jnp.float32)
+    done = (mid_ref[mine, :].astype(jnp.float32) + total).astype(jnp.bfloat16)
+    half_s[...] = done
+    out_ref[mine, :] = done
+    last = pltpu.make_async_remote_copy(
+        src_ref=half_s, dst_ref=half_r, send_sem=hs_sem, recv_sem=hr_sem,
+        device_id={"tp": 1 - core}, device_id_type=MESH,
+    )
+    last.start()
+    last.wait()
+    out_ref[other, :] = half_r[...]
+
+
+def layer_close(n, split, part, middle):
+    rows, width = middle.shape
+    half = rows // 2
+    vmem = pl.BlockSpec(memory_space=pltpu.VMEM)
+    dma = pltpu.SemaphoreType.DMA
+    bf16 = jnp.bfloat16
+    return pl.pallas_call(
+        functools.partial(close_kernel, n, split),
+        out_shape=jax.ShapeDtypeStruct((rows, width), bf16),
+        in_specs=[vmem] * 2,
+        out_specs=vmem,
+        scratch_shapes=[
+            pltpu.VMEM((split, half, width), bf16),
+            pltpu.VMEM((split - 1, half, width), bf16),
+            pltpu.VMEM((split - 1, half, width), bf16),
+            pltpu.VMEM((half, width), bf16),
+            pltpu.VMEM((half, width), bf16),
+            dma((split,)),
+            dma((split,)),
+            dma((split - 1,)),
+            dma((split - 1,)),
+            dma,
+            dma,
+        ],
+        compiler_params=pltpu.CompilerParams(
+            collective_id=2, has_side_effects=True, vmem_limit_bytes=24 << 20
+        ),
+        name="layer_close",
+    )(part, middle)
+
+
 def on_device(
     residual_in,
     mixer_input,
@@ -181,6 +632,47 @@
         mixer_input[:, length - LANES :], "sp", [(i, i + 1) for i in range(n - 1)]
     )
     rate = -8.0 * jax.nn.softplus(-decay_param)[:, None]
+    width, share_ff = residual_in.shape[1], gate_weight.shape[1]
+    split = 4
+    if (
+        lax.axis_size("tp") == 2
+        and n % split == 0
+        and n > split
+        and gate_weight.shape[0] % LANES == 0
+        and share_ff % (16 * split) == 0
+        and width % 512 == 0
+    ):
+        span = share_ff // split
+        packed = jnp.stack(
+            [
+                w.reshape(w.shape[0], split, span).transpose(1, 2, 0)
+                for w in (gate_weight, up_weight, down_weight)
+            ],
+            axis=1,
+        )
+        wide, tokens, middle = layer_front(
+            n,
+            split,
+            mixer_input,
+            halo,
+            branch_gate,
+            decay_extra,
+            conv_taps.astype(jnp.float32),
+            rate,
+            recur_weight.transpose(0, 2, 1),
+            admit_weight.transpose(0, 2, 1),
+            out_weight,
+            residual_in,
+            norm_gain.reshape(1, width),
+            packed,
+        )
+        tokens = tokens.reshape(-1, width)
+        across = (((1,), (1,)), ((), ()))
+        gate_pre = lax.dot_general(tokens, wide[0], across, preferred_element_type=jnp.float32)
+        up_pre = lax.dot_general(tokens, wide[1], across, preferred_element_type=jnp.float32)
+        hidden = (jax.nn.silu(gate_pre) * up_pre).astype(jnp.bfloat16)
+        part = jnp.dot(hidden, wide[2], preferred_element_type=jnp.float32).astype(jnp.bfloat16)
+        return layer_close(n, split, part.reshape(split, -1, width), middle)
     mixed_out = mixer(
         n,
         mixer_input,

time: 514 us -> 219 us (0.43)
  waiting for transfers between devices: 441 us -> 0.01 us
  Pallas kernels: 13.3 us -> 178 us
  between operations: 14.9 us -> 0.12 us
  matrix products: 27 us -> 18.7 us
  local copies, waits for them, and re-layouts: 8.49 us -> 16.6 us
    all_gather x4 -> x0, waiting for transfers between devices: 406 us -> none  [the longest x1 142 us: on_device(): down_whole = lax.all_gather(down_weight, 'sp', axis=0, tiled=True)]
    pallas_call x1 -> x2, Pallas kernels: 13.3 us -> 178 us  [the longest x1 124 us: layer_front(): pl.pallas_call(functools.partial(layer_kernel, n, split), out_shape=(jax....]
    psum x1 -> x0, waiting for transfers between devices: 20.8 us -> none  [on_device(): lax.psum(partial_value.astype(jnp.bfloat16), 'tp').astype(jnp.float32)]
    reduce_scatter x1 -> x0, waiting for transfers between devices: 9.23 us -> none  [on_device(): lax.psum_scatter(lax.dot_general(hidden, down_whole, (((1,), (1,)), ((),...]
    dot_general x3 -> x2, matrix products: 27 us -> 18.7 us  [the longest x1 12.2 us: on_device(): jnp.dot(hidden, wide[2], preferred_element_type=jnp.float32)]
    unnamed x15 -> x26, local copies, waits for them, and re-layouts: 5.6 us -> 13 us
  transfers between devices with their start and end apart: 7 -> 1, of which waited for: 7 -> 0; matrix products, arithmetic and copies ran while one was open for 3% -> 5% of each run, Pallas kernels for 0% -> 0%
where the time goes in v2:
time: 219 us
  Pallas kernels  178 us (81%)
  matrix products  18.7 us (9%)
  local copies, waits for them, and re-layouts  16.6 us (8%)
  starting transfers between devices  3.11 us (1%)
  other arithmetic  2.6 us (1%)
    pallas_call x1, Pallas kernels, layer_front(): pl.pallas_call(functools.partial(layer_kernel, n, split), out_shape=(jax....  124 us
    pallas_call x1, Pallas kernels, layer_close(): pl.pallas_call(functools.partial(close_kernel, n, split), out_shape=jax.S...  53.5 us
    unnamed x26, local copies, waits for them, and re-layouts  13 us
    dot_general x1, matrix products, on_device(): jnp.dot(hidden, wide[2], preferred_element_type=jnp.float32)  12.2 us
    dot_general x1, matrix products, on_device(): lax.dot_general(tokens, wide[1], across, preferred_element_type=jnp.float32)  6.53 us
  transfers between devices with their start and end apart: 1, of which 0 were waited for; matrix products, arithmetic and copies ran while one was open for 5% of the time, Pallas kernels for 0%

profile of v2, /device:TPU:25, one launch (start us, length us, event | category | flops | bytes accessed | tf_op | source)
XLA Modules:
  0.0 219.0 jit_solution(15274295793152100186)
XLA Ops:
  0.0 0.0 copy-start.8
  0.0 0.0 copy-start.9
  0.0 1.8 slice.12
  1.8 3.1 %collective-permute-start = (bf16[1024,128]{1,0:T(8,128)(2,1)}, bf16[1024,128]{1,0:T(8,128)(2,1)S(1)}, u32[]{:S(2)}, u32[]{:S(2)}) collective-permute-start(bf16[1024,128]{1,0:T(8,128)(2,1)} %slice.12), channel_id=1, source_target_pairs={{0,2},{2,4},{4,6},{6,8},{8,10},{10,12},{12,14},{14,16},{16,18},{18... | collective-permute-start | bytes 786440 | tf_op jit(solution)/shard_map/ppermute | solution.py:631
  4.9 0.7 fusion.13
  5.6 0.7 reshape.19.gain_ref
  6.3 1.1 copy.27
  7.4 1.1 copy.28
  8.5 0.2 copy.33.rate_ref
  8.8 0.9 copy.32.taps_ref
  9.7 0.0 copy-done.8
  9.7 1.1 copy.29
  10.8 0.0 copy-done.9
  10.8 1.1 copy.30
  11.9 0.0 copy-start.1
  11.9 0.0 copy-start.2
  12.0 2.4 %copy.31 = bf16[128,2816]{0,1:T(8,128)(2,1)} copy(bf16[128,2816]{1,0:T(8,128)(2,1)} %param.25) | data formatting | bytes 1441792 | tf_op args[12]
  14.3 0.0 copy-start.3
  14.3 0.0 copy-start.6
  14.3 1.9 pad_maximum_fusion.packed_ref
  16.2 0.0 collective-permute-done.halo_ref
  16.2 0.0 copy-done.1
  16.2 0.0 copy-done.2
  16.2 0.0 copy-done.3
  16.3 0.1 copy-done.6
  16.3 124.3 %layer_front.1 = (bf16[3,704,2048]{2,1,0:T(8,128)(2,1)}, bf16[4,256,2048]{2,1,0:T(8,128)(2,1)S(1)}, bf16[256,2048]{1,0:T(8,128)(2,1)S(1)}) custom-call(bf16[1024,256]{1,0:T(8,128)(2,1)S(1)} %copy-done.1, bf16[1024,128]{1,0:T(8,128)(2,1)S(1)} %collective-permute-done.halo_ref, bf16[1024,256]{1,0:T(8,128)(2,1)S(1)} %copy-done.6, f32[1024,256]{1,0:T(8,128)S(1)} %copy-done.2, ...), custom_call_target="tpu_custom_call" | custom-call | tf_op jit(solution)/shard_map/layer_front/pallas_call | solution.py:475
  140.6 0.0 copy-start.4
  140.6 1.0 copy-done.4
  141.6 0.0 copy-start.7
  141.6 2.0 copy-done.7
  143.6 6.5 %fusion.1 = f32[1024,704]{0,1:T(8,128)} fusion(bf16[1024,2048]{1,0:T(8,128)(2,1)S(1)} %bitcast.38, bf16[3,704,2048]{2,1,0:T(8,128)(2,1)} %get-tuple-element.9), kind=kOutput, calls=%fused_computation.2 | convolution fusion | flops 2952790016 | bytes 9961472 | tf_op jit(solution)/shard_map/dot_general | solution.py:672
  150.1 0.0 copy-start.5
  150.1 12.2 %convolution_convert_fusion = bf16[1024,2048]{1,0:T(8,128)(2,1)} fusion(bf16[3,704,2048]{2,1,0:T(8,128)(2,1)} %get-tuple-element.9, f32[1024,704]{0,1:T(8,128)} %fusion.1, bf16[1024,2048]{1,0:T(8,128)(2,1)} %bitcast.39), kind=kOutput, calls=%fused_computation | convolution fusion | flops 5912002560 | bytes 17039360 | tf_op jit(solution)/shard_map/dot_general | solution.py:674
  162.3 0.0 copy-done.5
  162.3 0.0 copy-start
  162.3 2.2 copy-done
  164.5 53.5 %layer_close.1 = bf16[256,2048]{1,0:T(8,128)(2,1)S(1)} custom-call(bf16[4,256,2048]{2,1,0:T(8,128)(2,1)S(1)} %bitcast.35, bf16[256,2048]{1,0:T(8,128)(2,1)S(1)} %copy-done.5), custom_call_target="tpu_custom_call" | custom-call | tf_op jit(solution)/shard_map/layer_close/pallas_call | solution.py:589
  218.0 1.0 copy.35
Async XLA Ops:
  0.0 9.7 %copy-start.8 = (bf16[128,2816]{1,0:T(8,128)(2,1)S(1)}, bf16[128,2816]{1,0:T(8,128)(2,1)}, u32[]{:S(2)}) copy-start(bf16[128,2816]{1,0:T(8,128)(2,1)} %param.23) | copy-start | bytes 2162692
  0.0 10.8 %copy-start.9 = (bf16[128,2816]{1,0:T(8,128)(2,1)S(1)}, bf16[128,2816]{1,0:T(8,128)(2,1)}, u32[]{:S(2)}) copy-start(bf16[128,2816]{1,0:T(8,128)(2,1)} %param.24) | copy-start | bytes 2162692
  1.8 14.4 %collective-permute-start = (bf16[1024,128]{1,0:T(8,128)(2,1)}, bf16[1024,128]{1,0:T(8,128)(2,1)S(1)}, u32[]{:S(2)}, u32[]{:S(2)}) collective-permute-start(bf16[1024,128]{1,0:T(8,128)(2,1)} %slice.12), channel_id=1, source_target_pairs={{0,2},{2,4},{4,6},{6,8},{8,10},{10,12},{12,14},{14,16},{16,18},{18... | collective-permute-start | bytes 786440 | tf_op jit(solution)/shard_map/ppermute | solution.py:631
  11.9 4.3 %copy-start.1 = (bf16[1024,256]{1,0:T(8,128)(2,1)S(1)}, bf16[1024,256]{1,0:T(8,128)(2,1)}, u32[]{:S(2)}) copy-start(bf16[1024,256]{1,0:T(8,128)(2,1)} %x_ref.1) | copy-start | bytes 1572868
  11.9 4.3 %copy-start.2 = (f32[1024,256]{1,0:T(8,128)S(1)}, f32[1024,256]{1,0:T(8,128)}, u32[]{:S(2)}) copy-start(f32[1024,256]{1,0:T(8,128)} %extra_ref.1) | copy-start | bytes 3145732
  14.3 1.9 copy-start.3
  14.3 2.0 copy-start.6
  140.6 1.0 copy-start.4
  141.6 2.0 copy-start.7
  150.1 12.2 %copy-start.5 = (bf16[256,2048]{1,0:T(8,128)(2,1)S(1)}, bf16[256,2048]{1,0:T(8,128)(2,1)}, u32[]{:S(2)}) copy-start(bf16[256,2048]{1,0:T(8,128)(2,1)} %copy-done.4) | copy-start | bytes 3145732
  162.3 2.2 copy-start

commit v3 on v2

--- a/solution.py
+++ b/solution.py
@@ -164,7 +164,6 @@
     n,
     split,
     x_ref,
-    halo_ref,
     bg_ref,
     extra_ref,
     taps_ref,
@@ -178,6 +177,7 @@
     wide_ref,
     tok_ref,
     mid_ref,
+    halo_ref,
     state_s,
     run_s,
     ends_s,
@@ -203,6 +203,10 @@
     cs_sem,
     cr_sem,
     own_sem,
+    hs_sem,
+    hr_sem,
+    rs_sem,
+    rr_sem,
 ):
     me = lax.axis_index("sp")
     core = lax.axis_index("tp")
@@ -247,15 +251,18 @@
             zs_sem.at[c, k - 1], zr_sem.at[c, k - 1], {"sp": source},
         )
 
+    def beside(m):
+        return spot + 1 - 2 * lax.rem(spot, 2) if m == 1 else spot + 2 - 4 * (spot // 2)
+
     def own_copy(c, m):
         return remote(
             packed_ref.at[rank, c], wide_ref.at[c, :, columns(me)],
             ps_sem.at[c, m - 1], pr_sem.at[c, m - 1],
-            {"sp": rank * plane + lax.rem(spot + m, plane)},
+            {"sp": rank * plane + beside(m)},
         )
 
     def own_landed(c, m):
-        source = rank * plane + lax.rem(spot - m + plane, plane)
+        source = rank * plane + beside(m)
         return remote(
             packed_ref.at[rank, c], wide_ref.at[c, :, columns(source)],
             ps_sem.at[c, m - 1], pr_sem.at[c, m - 1], {"sp": source},
@@ -266,17 +273,41 @@
         window = wide_ref.at[c, :, columns(source)]
         return remote(
             window, window, fs_sem.at[c, k - 1, m - 1], fr_sem.at[c, k - 1, m - 1],
-            {"sp": rank * plane + lax.rem(spot + m, plane)},
+            {"sp": rank * plane + beside(m)},
         )
 
     def pass_landed(c, k, m):
-        behind = lax.rem(spot - m + plane, plane)
+        behind = beside(m)
         source = lax.rem(rank - k + split, split) * plane + behind
         window = wide_ref.at[c, :, columns(source)]
         return remote(
             window, window, fs_sem.at[c, k - 1, m - 1], fr_sem.at[c, k - 1, m - 1],
             {"sp": rank * plane + behind},
         )
+
+    def relay_window(c, k, m, where):
+        source = lax.rem(rank - k + split, split) * plane + where
+        return wide_ref.at[c, pl.ds((m - 1) * (span // 2), span // 2), columns(source)]
+
+    def relay_copy(c, k, m):
+        window = relay_window(c, k, m, beside(m))
+        return remote(
+            window, window, rs_sem.at[c, k, m - 1], rr_sem.at[c, k, m - 1],
+            {"sp": rank * plane + beside(3 - m)},
+        )
+
+    def relay_landed(c, k, m):
+        window = relay_window(c, k, m, 3 - spot)
+        return remote(
+            window, window, rs_sem.at[c, k, m - 1], rr_sem.at[c, k, m - 1],
+            {"sp": rank * plane + beside(3 - m)},
+        )
+
+    def relay(c, k):
+        for m in (1, 2):
+            landed = pass_landed(c, k, m) if k else own_landed(c, m)
+            landed.wait_recv()
+            relay_copy(c, k, m).start()
 
     def z_start(c):
         for k in range(1, split):
@@ -285,15 +316,22 @@
     def z_pass(c):
         for k in range(1, split):
             z_landed(c, k).wait_recv()
-            for m in range(1, plane):
+            for m in (1, 2):
                 pass_copy(c, k, m).start()
 
+    halo_copy = remote(
+        x_ref.at[:, pl.ds(x_ref.shape[1] - LANES, LANES)], halo_ref, hs_sem, hr_sem,
+        {"sp": lax.rem(me + 1, n)},
+    )
+    halo_copy.start()
     z_start(0)
     for c in range(kinds):
-        for m in range(1, plane):
+        for m in (1, 2):
             own_copy(c, m).start()
     own_in = pltpu.make_async_copy(packed_ref.at[rank], own_s, own_sem.at[0])
     own_in.start()
+    halo_copy.wait()
+    inside = jnp.where(me > 0, 1.0, 0.0)
     channels, length = x_ref.shape
     block = wr_ref.shape[1]
     groups = channels // LANES
@@ -303,7 +341,7 @@
     def local(g, carry):
         rows = pl.ds(pl.multiple_of(g * LANES, LANES), LANES)
         wide = jnp.concatenate(
-            [halo_ref[rows, :].astype(jnp.float32), x_ref[rows, :].astype(jnp.float32)], axis=1
+            [halo_ref[rows, :].astype(jnp.float32) * inside, x_ref[rows, :].astype(jnp.float32)], axis=1
         )
         taps = taps_ref[rows, :]
         total = taps[:, tap_count - 1 :] * wide[:, LANES:]
@@ -338,6 +376,7 @@
     own_in.wait()
     own_out = pltpu.make_async_copy(own_s, wide_ref.at[:, :, columns(me)], own_sem.at[1])
     own_out.start()
+    relay(0, 0)
     z_pass(0)
     z_start(1)
     def copy_to(k):
@@ -439,7 +478,13 @@
         tok_copy(k).start()
     own_tok = pltpu.make_async_copy(nrm_s, tok_ref.at[rank], own_sem.at[2])
     own_tok.start()
+    relay(1, 0)
+    relay(2, 0)
+    for k in range(1, split):
+        relay(0, k)
     z_pass(2)
+    for k in range(1, split):
+        relay(1, k)
     for k in range(1, split):
         tok_landed(k).wait_recv()
         tok_pass(k, mine).start()
@@ -449,18 +494,22 @@
         tok_pass(k, other).wait_recv()
     own_tok.wait()
     own_out.wait()
+    for k in range(1, split):
+        relay(2, k)
     for c in range(kinds):
-        for m in range(1, plane):
+        for m in (1, 2):
             own_copy(c, m).wait_send()
-            own_landed(c, m).wait_recv()
-        for k in range(1, split):
-            z_copy(c, k).wait_send()
-            for m in range(1, plane):
-                pass_copy(c, k, m).wait_send()
-                pass_landed(c, k, m).wait_recv()
-
-
-def layer_front(n, split, x, halo, bg, extra, taps, rate, wr, wa, ow, res, gain, packed):
+        for k in range(split):
+            for m in (1, 2):
+                if k:
+                    pass_copy(c, k, m).wait_send()
+                relay_copy(c, k, m).wait_send()
+                relay_landed(c, k, m).wait_recv()
+            if k:
+                z_copy(c, k).wait_send()
+
+
+def layer_front(n, split, x, bg, extra, taps, rate, wr, wa, ow, res, gain, packed):
     channels, length = x.shape
     groups = channels // LANES
     rows, width = res.shape
@@ -479,9 +528,10 @@
             jax.ShapeDtypeStruct((split, rows, width), bf16),
             jax.ShapeDtypeStruct((rows, width), bf16),
         ),
-        in_specs=[vmem] * 11 + [hbm],
+        in_specs=[vmem] * 10 + [hbm],
         out_specs=(hbm, hbm, vmem),
         scratch_shapes=[
+            pltpu.VMEM((channels, LANES), bf16),
             pltpu.VMEM((channels, length), f32),
             pltpu.VMEM((channels, length), f32),
             pltpu.VMEM((2 * groups, LANES), f32),
@@ -496,10 +546,10 @@
             dma((n - 1,)),
             dma((kinds, split - 1)),
             dma((kinds, split - 1)),
-            dma((kinds, plane - 1)),
-            dma((kinds, plane - 1)),
-            dma((kinds, split - 1, plane - 1)),
-            dma((kinds, split - 1, plane - 1)),
+            dma((kinds, 2)),
+            dma((kinds, 2)),
+            dma((kinds, split - 1, 2)),
+            dma((kinds, split - 1, 2)),
             dma((split - 1,)),
             dma((split - 1,)),
             dma((pieces,)),
@@ -507,17 +557,21 @@
             dma((split - 1,)),
             dma((split - 1,)),
             dma((3,)),
+            dma,
+            dma,
+            dma((kinds, split, 2)),
+            dma((kinds, split, 2)),
         ],
         compiler_params=pltpu.CompilerParams(
             collective_id=1, has_side_effects=True, vmem_limit_bytes=40 << 20
         ),
         name="layer_front",
-    )(x, halo, bg, extra, taps, rate, wr, wa, ow, res, gain, packed)
+    )(x, bg, extra, taps, rate, wr, wa, ow, res, gain, packed)
 
 
 def close_kernel(
-    n, split, part_ref, mid_ref, out_ref,
-    tp_s, red_s, z_s, half_s, half_r,
+    n, split, tok_ref, wide_ref, mid_ref, out_ref,
+    part_ref, tok_s, wide_s, tk_sem, wd_sem, tp_s, red_s, z_s, half_s, half_r,
     as_sem, ar_sem, zs_sem, zr_sem, hs_sem, hr_sem,
 ):
     me = lax.axis_index("sp")
@@ -525,14 +579,45 @@
     plane = n // split
     rank, spot = me // plane, lax.rem(me, plane)
     barrier = pltpu.get_barrier_semaphore()
+    order = list(range(1, split)) + [0]
+    kinds = wide_ref.shape[0]
+
+    def tok_in(k):
+        return pltpu.make_async_copy(
+            tok_ref.at[lax.rem(rank + k, split)], tok_s.at[k], tk_sem.at[k]
+        )
+
+    def wide_in(c):
+        return pltpu.make_async_copy(wide_ref.at[c], wide_s.at[c], wd_sem.at[c])
+
+    tok_in(order[0]).start()
+    for c in range(kinds):
+        wide_in(c).start()
+    for k in order[1:]:
+        tok_in(k).start()
     for k in range(1, split):
         pl.semaphore_signal(
             barrier, inc=1,
             device_id={"sp": lax.rem(rank + k, split) * plane + spot}, device_id_type=MESH,
         )
     pl.semaphore_signal(barrier, inc=1, device_id={"tp": 1 - core}, device_id_type=MESH)
-    pl.semaphore_wait(barrier, split)
-    half = part_ref.shape[1] // 2
+    def feed(k):
+        tok_in(k).wait()
+        across = (((1,), (1,)), ((), ()))
+        if k == order[0]:
+            wide_in(0).wait()
+        gate = lax.dot_general(tok_s[k], wide_s[0], across, preferred_element_type=jnp.float32)
+        if k == order[0]:
+            wide_in(1).wait()
+        up = lax.dot_general(tok_s[k], wide_s[1], across, preferred_element_type=jnp.float32)
+        hidden = (gate / (1.0 + jnp.exp(-gate)) * up).astype(jnp.bfloat16)
+        if k == order[0]:
+            wide_in(2).wait()
+        part_ref[k] = jnp.dot(
+            hidden, wide_s[2], preferred_element_type=jnp.float32
+        ).astype(jnp.bfloat16)
+
+    half = mid_ref.shape[0] // 2
     mine = pl.ds(pl.multiple_of(core * half, half), half)
     other = pl.ds(pl.multiple_of((1 - core) * half, half), half)
 
@@ -541,7 +626,7 @@
 
     def tp_copy(k):
         return pltpu.make_async_remote_copy(
-            src_ref=part_ref.at[to_rank(k), other, :], dst_ref=tp_s.at[k],
+            src_ref=part_ref.at[k, other, :], dst_ref=tp_s.at[k],
             send_sem=as_sem.at[k], recv_sem=ar_sem.at[k],
             device_id={"tp": 1 - core}, device_id_type=MESH,
         )
@@ -553,18 +638,25 @@
             device_id={"sp": to_rank(k) * plane + spot}, device_id_type=MESH,
         )
 
-    order = list(range(1, split)) + [0]
-    for k in order:
+    def reduce(k):
+        tp_copy(k).wait()
+        mixed = part_ref[k, mine, :].astype(jnp.float32) + tp_s[k].astype(jnp.float32)
+        red_s[k - 1] = mixed.astype(jnp.bfloat16)
+
+    feed(1)
+    pl.semaphore_wait(barrier, split)
+    tp_copy(1).start()
+    for k in range(2, split):
+        feed(k)
         tp_copy(k).start()
-    for k in order[:-1]:
-        tp_copy(k).wait()
-        mixed = part_ref[to_rank(k), mine, :].astype(jnp.float32) + tp_s[k].astype(jnp.float32)
-        red_s[k - 1] = mixed.astype(jnp.bfloat16)
-        if k > 1:
-            z_copy(k - 1).start()
+        reduce(k - 1)
+        z_copy(k - 1).start()
+    reduce(split - 1)
+    z_copy(split - 1).start()
+    feed(0)
+    tp_copy(0).start()
     tp_copy(0).wait()
-    z_copy(split - 1).start()
-    total = part_ref[rank, mine, :].astype(jnp.float32) + tp_s[0].astype(jnp.float32)
+    total = part_ref[0, mine, :].astype(jnp.float32) + tp_s[0].astype(jnp.float32)
     for k in range(1, split):
         z_copy(k).wait()
         total = total + z_s[k - 1].astype(jnp.float32)
@@ -580,7 +672,7 @@
     out_ref[other, :] = half_r[...]
 
 
-def layer_close(n, split, part, middle):
+def layer_close(n, split, tokens, wide, middle):
     rows, width = middle.shape
     half = rows // 2
     vmem = pl.BlockSpec(memory_space=pltpu.VMEM)
@@ -589,9 +681,14 @@
     return pl.pallas_call(
         functools.partial(close_kernel, n, split),
         out_shape=jax.ShapeDtypeStruct((rows, width), bf16),
-        in_specs=[vmem] * 2,
+        in_specs=[pl.BlockSpec(memory_space=pl.ANY)] * 2 + [vmem],
         out_specs=vmem,
         scratch_shapes=[
+            pltpu.VMEM((split, rows, width), bf16),
+            pltpu.VMEM((split, rows, width), bf16),
+            pltpu.VMEM(wide.shape, bf16),
+            dma((split,)),
+            dma((wide.shape[0],)),
             pltpu.VMEM((split, half, width), bf16),
             pltpu.VMEM((split - 1, half, width), bf16),
             pltpu.VMEM((split - 1, half, width), bf16),
@@ -605,10 +702,10 @@
             dma,
         ],
         compiler_params=pltpu.CompilerParams(
-            collective_id=2, has_side_effects=True, vmem_limit_bytes=24 << 20
+            collective_id=2, has_side_effects=True, vmem_limit_bytes=48 << 20
         ),
         name="layer_close",
-    )(part, middle)
+    )(tokens, wide, middle)
 
 
 def on_device(
@@ -636,10 +733,9 @@
     split = 4
     if (
         lax.axis_size("tp") == 2
-        and n % split == 0
-        and n > split
+        and n == 4 * split
         and gate_weight.shape[0] % LANES == 0
-        and share_ff % (16 * split) == 0
+        and share_ff % (32 * split) == 0
         and width % 512 == 0
     ):
         span = share_ff // split
@@ -654,7 +750,6 @@
             n,
             split,
             mixer_input,
-            halo,
             branch_gate,
             decay_extra,
             conv_taps.astype(jnp.float32),
@@ -666,13 +761,7 @@
             norm_gain.reshape(1, width),
             packed,
         )
-        tokens = tokens.reshape(-1, width)
-        across = (((1,), (1,)), ((), ()))
-        gate_pre = lax.dot_general(tokens, wide[0], across, preferred_element_type=jnp.float32)
-        up_pre = lax.dot_general(tokens, wide[1], across, preferred_element_type=jnp.float32)
-        hidden = (jax.nn.silu(gate_pre) * up_pre).astype(jnp.bfloat16)
-        part = jnp.dot(hidden, wide[2], preferred_element_type=jnp.float32).astype(jnp.bfloat16)
-        return layer_close(n, split, part.reshape(split, -1, width), middle)
+        return layer_close(n, split, tokens, wide, middle)
     mixed_out = mixer(
         n,
         mixer_input,

time: 219 us -> 196 us (0.89)
  matrix products: 18.7 us -> 0 us
  local copies, waits for them, and re-layouts: 16.6 us -> 11.6 us
  Pallas kernels: 178 us -> 182 us
  starting transfers between devices: 3.11 us -> 0 us
    dot_general x2 -> x0, matrix products: 18.7 us -> none  [the longest x1 12.2 us: on_device(): jnp.dot(hidden, wide[2], preferred_element_type=jnp.float32)]
    pallas_call x1, Pallas kernels: 53.5 us -> 59 us  [layer_close(): pl.pallas_call(functools.partial(close_kernel, n, split), out_shape=jax.S...]
    unnamed x26 -> x18, local copies, waits for them, and re-layouts: 13 us -> 9.76 us
    ppermute x1 -> x0, starting transfers between devices: 3.11 us -> none  [on_device(): lax.ppermute(mixer_input[:, length - LANES:], 'sp', [(i, i + 1) for i in...]
  transfers between devices with their start and end apart: 1 -> 0, of which waited for: 0 -> 0; matrix products, arithmetic and copies ran while one was open for 5% -> 0% of each run, Pallas kernels for 0% -> 0%
where the time goes in v3:
time: 196 us; the launch traced here: 195 us
  Pallas kernels  182 us (93%)
  local copies, waits for them, and re-layouts  11.6 us (6%)
  other arithmetic  2.27 us (1%)
    pallas_call x1, Pallas kernels, layer_front(): pl.pallas_call(functools.partial(layer_kernel, n, split), out_shape=(jax....  123 us
    pallas_call x1, Pallas kernels, layer_close(): pl.pallas_call(functools.partial(close_kernel, n, split), out_shape=jax.S...  59 us
    unnamed x18, local copies, waits for them, and re-layouts  9.76 us

profile of v3, /device:TPU:25, one launch (start us, length us, event | category | flops | bytes accessed | tf_op | source)
XLA Modules:
  0.0 195.4 jit_solution(4351270999682735000)
XLA Ops:
  0.0 0.0 copy-start.5
  0.0 0.8 fusion
  0.8 0.7 reshape.13.gain_ref
  1.5 1.1 copy.27
  2.6 1.1 copy.28
  3.7 0.2 copy.33.rate_ref
  3.9 0.9 copy.32.taps_ref
  4.8 0.0 copy-done.5
  4.8 0.3 copy.29
  5.2 1.5 copy.30
  6.6 2.2 %copy.31 = bf16[128,2816]{0,1:T(8,128)(2,1)} copy(bf16[128,2816]{1,0:T(8,128)(2,1)} %param.25) | data formatting | bytes 1441792 | tf_op args[12]
  8.9 0.0 copy-start.1
  8.9 0.0 copy-start.2
  8.9 0.0 copy-start.3
  8.9 0.0 copy-start.4
  8.9 1.5 pad_maximum_fusion.packed_ref
  10.4 0.0 copy-done.1
  10.4 0.2 copy-done.2
  10.7 0.1 copy-done.3
  10.8 0.2 copy-done.4
  10.9 122.5 %layer_front.1 = (bf16[3,704,2048]{2,1,0:T(8,128)(2,1)}, bf16[4,256,2048]{2,1,0:T(8,128)(2,1)S(1)}, bf16[256,2048]{1,0:T(8,128)(2,1)S(1)}) custom-call(bf16[1024,256]{1,0:T(8,128)(2,1)S(1)} %copy-done.3, bf16[1024,256]{1,0:T(8,128)(2,1)S(1)} %copy-done.4, f32[1024,256]{1,0:T(8,128)S(1)} %copy-done.1, f32[1024,4]{1,0:T(8,128)S(1)} %copy.32.taps_ref, ...), custom_call_target="tpu_custom_call" | custom-call | tf_op jit(solution)/shard_map/layer_front/pallas_call | solution.py:524
  133.5 0.0 copy-start
  133.5 2.0 %copy-done = bf16[4,256,2048]{2,1,0:T(8,128)(2,1)} copy-done((bf16[4,256,2048]{2,1,0:T(8,128)(2,1)}, bf16[4,256,2048]{2,1,0:T(8,128)(2,1)S(1)}, u32[]{:S(2)}) %copy-start) | copy-done | bytes 4194328
  135.5 59.0 %layer_close.1 = bf16[256,2048]{1,0:T(8,128)(2,1)S(1)} custom-call(bf16[4,256,2048]{2,1,0:T(8,128)(2,1)} %copy-done, bf16[3,704,2048]{2,1,0:T(8,128)(2,1)} %get-tuple-element.9.wide_ref, bf16[256,2048]{1,0:T(8,128)(2,1)S(1)} %get-tuple-element.10.mid_ref), custom_call_target="tpu_custom_call" | custom-call | tf_op jit(solution)/shard_map/layer_close/pallas_call | solution.py:681
  194.5 1.0 copy.35
Async XLA Ops:
  0.0 4.8 %copy-start.5 = (bf16[128,2816]{1,0:T(8,128)(2,1)S(1)}, bf16[128,2816]{1,0:T(8,128)(2,1)}, u32[]{:S(2)}) copy-start(bf16[128,2816]{1,0:T(8,128)(2,1)} %param.23) | copy-start | bytes 2162692
  8.9 1.5 copy-start.1
  8.9 1.8 copy-start.2
  8.9 1.9 copy-start.3
  8.9 2.0 %copy-start.4 = (bf16[1024,256]{1,0:T(8,128)(2,1)S(1)}, bf16[1024,256]{1,0:T(8,128)(2,1)}, u32[]{:S(2)}) copy-start(bf16[1024,256]{1,0:T(8,128)(2,1)} %bg_ref.1) | copy-start | bytes 1572868
  133.5 2.0 %copy-start = (bf16[4,256,2048]{2,1,0:T(8,128)(2,1)}, bf16[4,256,2048]{2,1,0:T(8,128)(2,1)S(1)}, u32[]{:S(2)}) copy-start(bf16[4,256,2048]{2,1,0:T(8,128)(2,1)S(1)} %get-tuple-element.8.tok_ref) | copy-start | bytes 12582916
